TPU v7x, 32 devices: a whole 2x2x4 slice. The times are simulated.
32 devices in a mesh: ra: 8 (over z, y), cb: 4 (over x, core).
Axes of the slice: x: 2, y: 2, z: 4, core: 2. Of those that a mesh axis runs over, the one named last changes fastest.
Arguments:
- tokens: bfloat16 [2048, 4096], P('ra'), may hold values from -16 to 16
- norm_gain: float32 [2, 2048], replicated, may hold values from 0.1 to 1.9
- up_weight: float32 [2, 2048, 6144], P(None, 'ra', 'cb'), may hold values from -0.125 to 0.125
- gate_weight: float32 [2, 2048, 6144], P(None, 'ra', 'cb'), may hold values from -0.125 to 0.125
- up_scale: float32 [2, 6144], P(None, 'cb'), may hold values from 0.5 to 2
- gate_scale: float32 [2, 6144], P(None, 'cb'), may hold values from 0.5 to 2
- up_taps: float32 [2, 3, 6144], P(None, None, 'cb'), may hold values from -3 to 3
- gate_taps: float32 [2, 3, 6144], P(None, None, 'cb'), may hold values from -3 to 3
- down_weight: float32 [2, 2048, 6144], P(None, 'ra', 'cb'), may hold values from -0.078125 to 0.078125
- down_scale: float32 [2, 2048], replicated, may hold values from 0.5 to 2
Outputs:
- mixed: bfloat16 [2048, 4096], P('ra')
All inputs are finite; a program needn't handle non-finite values.
Results may differ from a plain program's by a relative error of at most 0.024.
Values may be sent and summed in bfloat16 or wider, within the bound.
A program may use at most 128 MiB of HBM per device.

v0:
```python
import jax
import jax.numpy as jnp
from jax import lax
from jax.sharding import PartitionSpec as P

EPS = 1e-06
RESIDUAL = 0.5


def shifted(value, axis, steps):
    count = lax.axis_size(axis)
    initial, last = (max(0, -steps), min(count, count - steps))
    return lax.ppermute(value, axis, [(source, source + steps) for source in range(initial, last)])


def valid_taps(values, taps):
    width = taps.shape[0]
    length = values.shape[0] - width + 1
    total = taps[0][None, :] * values[0:length]
    for k in range(1, width):
        total = total + taps[k][None, :] * values[k : k + length]
    return total


def per_device(
    tokens,
    norm_gain,
    up_weight,
    gate_weight,
    up_scale,
    gate_scale,
    up_taps,
    gate_taps,
    down_weight,
    down_scale,
):
    state = lax.all_to_all(tokens, "ra", split_axis=1, concat_axis=0, tiled=True).T
    edge = up_taps.shape[1] - 1
    for layer in range(up_weight.shape[0]):
        rows = state
        rows_f = rows.astype(jnp.float32)
        inverse = lax.rsqrt(jnp.mean(rows_f * rows_f, axis=1, keepdims=True) + EPS)
        scaled = (rows_f * norm_gain[layer][None, :]).astype(jnp.bfloat16)
        up_raw = jnp.dot(
            scaled,
            lax.all_gather(up_weight[layer].astype(jnp.bfloat16), "ra", axis=0, tiled=True),
            preferred_element_type=jnp.float32,
        )
        gate_raw = jnp.dot(
            scaled,
            lax.all_gather(gate_weight[layer].astype(jnp.bfloat16), "ra", axis=0, tiled=True),
            preferred_element_type=jnp.float32,
        )
        up_pre = up_raw * inverse * up_scale[layer][None, :]
        gate_pre = gate_raw * inverse * gate_scale[layer][None, :]
        prev_up, prev_gate = shifted(
            (up_pre[up_pre.shape[0] - edge :], gate_pre[gate_pre.shape[0] - edge :]), "ra", 1
        )
        up_pre = jnp.concatenate([prev_up, up_pre], axis=0)
        gate_pre = jnp.concatenate([prev_gate, gate_pre], axis=0)
        conv_up = valid_taps(up_pre, up_taps[layer])
        conv_gate = valid_taps(gate_pre, gate_taps[layer])
        hidden = (jax.nn.silu(conv_gate) * conv_up).astype(jnp.bfloat16)
        down_part = lax.dot_general(
            hidden,
            lax.all_gather(down_weight[layer].astype(jnp.bfloat16), "ra", axis=0, tiled=True),
            (((1,), (1,)), ((), ())),
            preferred_element_type=jnp.float32,
        )
        down = lax.psum(down_part.astype(jnp.bfloat16), "cb").astype(jnp.float32)
        state = (down * down_scale[layer][None, :] + RESIDUAL * state.astype(jnp.float32)).astype(
            jnp.bfloat16
        )
    return lax.all_to_all(state.T, "ra", split_axis=0, concat_axis=1, tiled=True)


def solution(mesh):
    placed = (
        P("ra", None),
        P(),
        P(None, "ra", "cb"),
        P(None, "ra", "cb"),
        P(None, "cb"),
        P(None, "cb"),
        P(None, None, "cb"),
        P(None, None, "cb"),
        P(None, "ra", "cb"),
        P(),
    )
    return jax.shard_map(
        per_device, mesh=mesh, in_specs=placed, out_specs=P("ra", None), check_vma=False
    )
```

profile of v0, /device:TPU:0, one launch (start us, length us, event | category | flops | bytes accessed | tf_op | source)
XLA Modules:
  0.0 837.4 jit_solution(4904350089643967842)
XLA Ops:
  6.5 2.1 convert.14
  8.6 1.4 fusion.80
  10.0 0.0 all-gather.15.cloned.1.call-start
  10.0 1.0 copy-done.1
  11.1 0.2 convert.15
  11.3 1.3 fusion.81
  12.6 1.1 copy-done.2
  13.7 0.2 convert.16
  13.9 1.3 fusion.82
  15.2 0.8 copy-done.3
  16.0 2.4 copy.13
  18.5 7.4 all-to-all-start
  26.1 97.0 %all-to-all-done = bf16[256,8,512]{0,2,1:T(8,128)(2,1)S(1)} async-done(((bf16[256,8,512]{0,2,1:T(8,128)(2,1)}), bf16[256,8,512]{0,2,1:T(8,128)(2,1)S(1)}, u32[]{:S(2)}, u32[]{:S(2)}) %all-to-all-start) | async-done | bytes 2097184 | tf_op jit(solution)/shard_map/all_to_all | solution.py:37
  123.1 0.4 convert_bitcast_fusion
  123.4 0.6 copy.18
  124.1 2.0 copy-done
  126.1 0.3 multiply_reduce_fusion
  126.5 21.8 %all-gather.13.cloned.1.call-done = bf16[1,2048,1536]{2,1,0:T(8,128)(2,1)} async-done(((bf16[1,256,1536]{2,1,0:T(8,128)(2,1)}), bf16[1,2048,1536]{2,1,0:T(8,128)(2,1)}) %all-gather.13.cloned.1.call-update) | async-done | bytes 6291472 | tf_op jit(solution)/shard_map/all_gather | solution.py:51
  148.3 6.8 fusion.20
  155.1 1.7 copy-done.10
  156.8 1.7 collective-permute-start
  158.5 88.0 %all-gather.15.cloned.1.call-done = bf16[1,2048,1536]{2,1,0:T(8,128)(2,1)} async-done(((bf16[1,256,1536]{2,1,0:T(8,128)(2,1)}), bf16[1,2048,1536]{2,1,0:T(8,128)(2,1)}) %all-gather.15.cloned.1.call-update) | async-done | bytes 6291472 | tf_op jit(solution)/shard_map/all_gather | solution.py:46
  246.5 6.8 fusion.26
  253.3 2.5 collective-permute-start.1
  255.8 0.2 slice_reduce_fusion.3
  256.0 89.7 %all-gather.17.cloned.1.call-done = bf16[1,2048,1536]{2,1,0:T(8,128)(2,1)} async-done(((bf16[1,256,1536]{2,1,0:T(8,128)(2,1)}), bf16[1,2048,1536]{2,1,0:T(8,128)(2,1)}) %all-gather.17.cloned.1.call-update) | async-done | bytes 6291472 | tf_op jit(solution)/shard_map/all_gather | solution.py:66
  345.7 13.5 %fusion.65 = bf16[512,2048]{1,0:T(8,128)(2,1)} fusion(bf16[1,2048,1536]{2,1,0:T(8,128)(2,1)} %all-gather.17.cloned.1.call-done, f32[2,1536]{1,0:T(2,128)S(1)} %collective-permute-done.1, f32[512,1536]{1,0:T(8,128)} %copy-done.12, f32[512,1536]{1,0:T(8,128)} %copy-done.10, f32[2,1536]{1,0:T(2,128)S(1)} %collective-permute-done, ...), kind=kOutput, calls=%fused_computation.68 | convolution fusion | flops 3238002688 | bytes 14741504 | tf_op jit(solution)/shard_map/dot_general | solution.py:64
  359.2 0.0 all-gather.19.cloned.1.call-start
  359.3 0.5 all-gather.19.cloned.1.call-update
  359.8 0.5 all-gather.21.cloned.1.call-update
  360.4 0.7 all-gather.23.cloned.1.call-update
  361.2 47.7 %all-reduce.3.cloned.1.call-done = bf16[512,2048]{1,0:T(8,128)(2,1)} async-done(((bf16[512,2048]{1,0:T(8,128)(2,1)}), bf16[512,2048]{1,0:T(8,128)(2,1)}) %all-reduce.3.cloned.1.call-update) | async-done | bytes 2097168 | tf_op jit(solution)/shard_map/psum | solution.py:70
  408.9 4.0 fusion.13
  413.0 96.8 %all-gather.19.cloned.1.call-done = bf16[1,2048,1536]{2,1,0:T(8,128)(2,1)} async-done(((bf16[1,256,1536]{2,1,0:T(8,128)(2,1)}), bf16[1,2048,1536]{2,1,0:T(8,128)(2,1)}) %all-gather.19.cloned.1.call-update) | async-done | bytes 6291472 | tf_op jit(solution)/shard_map/all_gather | solution.py:51
  509.7 5.5 fusion.32
  515.3 1.6 copy-done.11
  516.9 2.6 collective-permute-start.2
  519.6 89.3 %all-gather.21.cloned.1.call-done = bf16[1,2048,1536]{2,1,0:T(8,128)(2,1)} async-done(((bf16[1,256,1536]{2,1,0:T(8,128)(2,1)}), bf16[1,2048,1536]{2,1,0:T(8,128)(2,1)}) %all-gather.21.cloned.1.call-update) | async-done | bytes 6291472 | tf_op jit(solution)/shard_map/all_gather | solution.py:46
  608.8 5.5 fusion.38
  614.4 1.6 copy-done.13
  616.0 2.5 collective-permute-start.3
  618.5 89.6 %all-gather.23.cloned.1.call-done = bf16[1,2048,1536]{2,1,0:T(8,128)(2,1)} async-done(((bf16[1,256,1536]{2,1,0:T(8,128)(2,1)}), bf16[1,2048,1536]{2,1,0:T(8,128)(2,1)}) %all-gather.23.cloned.1.call-update) | async-done | bytes 6291472 | tf_op jit(solution)/shard_map/all_gather | solution.py:66
  708.0 13.9 %fusion.68 = bf16[512,2048]{1,0:T(8,128)(2,1)} fusion(bf16[1,2048,1536]{2,1,0:T(8,128)(2,1)} %all-gather.23.cloned.1.call-done, f32[2,1536]{1,0:T(2,128)S(1)} %collective-permute-done.3, f32[512,1536]{1,0:T(8,128)} %copy-done.13, f32[512,1536]{1,0:T(8,128)} %copy-done.11, f32[2,1536]{1,0:T(2,128)S(1)} %collective-permute-done.2, ...), kind=kOutput, calls=%fused_computation.69 | convolution fusion | flops 3238002688 | bytes 14741504 | tf_op jit(solution)/shard_map/dot_general | solution.py:64
  722.0 49.7 %all-reduce.5.cloned.1.call-done = bf16[512,2048]{1,0:T(8,128)(2,1)} async-done(((bf16[512,2048]{1,0:T(8,128)(2,1)}), bf16[512,2048]{1,0:T(8,128)(2,1)}) %all-reduce.5.cloned.1.call-update) | async-done | bytes 2097168 | tf_op jit(solution)/shard_map/psum | solution.py:70
  771.7 2.5 fusion.15
  774.2 0.1 copy.20
  774.3 53.4 %all_to_all.32 = bf16[8,256,512]{1,2,0:T(8,128)(2,1)S(1)} all-to-all(bf16[8,256,512]{1,2,0:T(8,128)(2,1)S(1)} %bitcast.66), channel_id=1, replica_groups=mesh['ra'=8,'cb'=4] {'ra'}, dimensions={0} | all-to-all | bytes 4194304 | tf_op jit(solution)/shard_map/all_to_all | solution.py:74
  827.7 2.8 copy.16
  (46 shorter events, 0.5 us)
Async XLA Ops:
  6.5 141.7 %all-gather.13.cloned.1.call-start = ((), (), s32[]{:S(2)}) async-start(), calls=%async_computation.4 | async-start | bytes 7077888 | tf_op jit(solution)/shard_map/all_gather | solution.py:51
  8.6 2.5 copy-start.1
  10.0 236.5 %all-gather.15.cloned.1.call-start = ((), (), s32[]{:S(2)}) async-start(), calls=%async_computation.5 | async-start | bytes 7077888 | tf_op jit(solution)/shard_map/all_gather | solution.py:46
  11.2 2.5 copy-start.2
  12.6 333.1 %all-gather.17.cloned.1.call-start = ((), (), s32[]{:S(2)}) async-start(), calls=%async_computation.6 | async-start | bytes 7077888 | tf_op jit(solution)/shard_map/all_gather | solution.py:66
  13.9 2.2 copy-start.3
  18.5 7.5 copy-start.8
  18.5 7.5 copy-start.9
  18.5 7.6 copy-start.6
  18.5 104.6 %all-to-all-start = ((bf16[256,8,512]{0,2,1:T(8,128)(2,1)}), bf16[256,8,512]{0,2,1:T(8,128)(2,1)S(1)}, u32[]{:S(2)}, u32[]{:S(2)}) async-start(bf16[256,8,512]{0,2,1:T(8,128)(2,1)} %bitcast.64), calls=%async_computation | async-start | bytes 4194304 | tf_op jit(solution)/shard_map/all_to_all | solution.py:37
  25.9 383.0 %all-reduce.3.cloned.1.call-start = ((), (), s32[]{:S(2)}) async-start(), calls=%async_computation.2 | async-start | bytes 4194304 | tf_op jit(solution)/shard_map/psum | solution.py:70
  124.1 2.0 copy-start
  155.1 1.7 copy-start.10
  156.8 188.9 %collective-permute-start = (f32[2,1536]{1,0:T(2,128)S(1)}, f32[2,1536]{1,0:T(2,128)S(1)}, u32[]{:S(2)}, u32[]{:S(2)}) collective-permute-start(f32[2,1536]{1,0:T(2,128)S(1)} %slice.187), channel_id=1, source_target_pairs={{0,4},{4,8},{8,12},{12,16},{16,20},{20,24},{24,28},{1,5},{5,9},{9,... | collective-permute-start | bytes 36872 | tf_op jit(solution)/shard_map/ppermute | solution.py:13
  246.5 9.3 %copy-start.4 = (f32[2,3,1536]{2,0,1:T(2,128)S(1)}, f32[2,3,1536]{2,0,1:T(2,128)}, u32[]{:S(2)}) copy-start(f32[2,3,1536]{2,0,1:T(2,128)} %param.16) | copy-start | bytes 110596
  246.5 9.3 %copy-start.5 = (f32[2,3,1536]{2,0,1:T(2,128)S(1)}, f32[2,3,1536]{2,0,1:T(2,128)}, u32[]{:S(2)}) copy-start(f32[2,3,1536]{2,0,1:T(2,128)} %param.17) | copy-start | bytes 110596
  253.3 2.5 copy-start.12
  253.3 92.3 %collective-permute-start.1 = (f32[2,1536]{1,0:T(2,128)S(1)}, f32[2,1536]{1,0:T(2,128)S(1)}, u32[]{:S(2)}, u32[]{:S(2)}) collective-permute-start(f32[2,1536]{1,0:T(2,128)S(1)} %slice.191), channel_id=1, source_target_pairs={{0,4},{4,8},{8,12},{12,16},{16,20},{20,24},{24,28},{1,5},{5,9},{9,... | collective-permute-start | bytes 36872 | tf_op jit(solution)/shard_map/ppermute | solution.py:13
  359.2 2.0 copy-start.7
  359.2 150.5 %all-gather.19.cloned.1.call-start = ((), (), s32[]{:S(2)}) async-start(), calls=%async_computation.7 | async-start | bytes 7077888 | tf_op jit(solution)/shard_map/all_gather | solution.py:51
  359.8 249.0 %all-gather.21.cloned.1.call-start = ((), (), s32[]{:S(2)}) async-start(), calls=%async_computation.8 | async-start | bytes 7077888 | tf_op jit(solution)/shard_map/all_gather | solution.py:46
  360.4 347.7 %all-gather.23.cloned.1.call-start = ((), (), s32[]{:S(2)}) async-start(), calls=%async_computation.9 | async-start | bytes 7077888 | tf_op jit(solution)/shard_map/all_gather | solution.py:66
  361.1 410.6 %all-reduce.5.cloned.1.call-start = ((), (), s32[]{:S(2)}) async-start(), calls=%async_computation.3 | async-start | bytes 4194304 | tf_op jit(solution)/shard_map/psum | solution.py:70
  515.3 1.6 copy-start.11
  516.9 191.1 %collective-permute-start.2 = (f32[2,1536]{1,0:T(2,128)S(1)}, f32[2,1536]{1,0:T(2,128)S(1)}, u32[]{:S(2)}, u32[]{:S(2)}) collective-permute-start(f32[2,1536]{1,0:T(2,128)S(1)} %slice.196), channel_id=1, source_target_pairs={{0,4},{4,8},{8,12},{12,16},{16,20},{20,24},{24,28},{1,5},{5,9},{9,... | collective-permute-start | bytes 36872 | tf_op jit(solution)/shard_map/ppermute | solution.py:13
  614.4 1.6 copy-start.13
  616.0 92.0 %collective-permute-start.3 = (f32[2,1536]{1,0:T(2,128)S(1)}, f32[2,1536]{1,0:T(2,128)S(1)}, u32[]{:S(2)}, u32[]{:S(2)}) collective-permute-start(f32[2,1536]{1,0:T(2,128)S(1)} %slice.200), channel_id=1, source_target_pairs={{0,4},{4,8},{8,12},{12,16},{16,20},{20,24},{24,28},{1,5},{5,9},{9,... | collective-permute-start | bytes 36872 | tf_op jit(solution)/shard_map/ppermute | solution.py:13
Sparse Core Ops, SparseCore 0:
  10.1 138.1 all-gather.12
  150.5 96.0 all-gather.14
  248.7 96.9 all-gather.16
  359.3 49.5 all-reduce.2
  410.9 98.7 all-gather.18
  511.8 96.9 all-gather.20
  611.0 96.9 all-gather.22
  722.1 49.5 all-reduce.4
where the time goes:
time: 838 us; the launch traced here: 837 us
  waiting for transfers between devices  671 us (80%)
  blocking collectives  53.4 us (6%)
  matrix products  52 us (6%)
  local copies, waits for them, and re-layouts  20.3 us (2%)
  starting transfers between devices  17 us (2%)
  between operations  13.8 us (2%)
  other arithmetic  9.65 us (1%)
    all_gather x2, waiting for transfers between devices, per_device(): lax.all_gather(down_weight[layer].astype(jnp.bfloat16), 'ra', axis=0, til...  179 us
    all_gather x2, waiting for transfers between devices, per_device(): lax.all_gather(up_weight[layer].astype(jnp.bfloat16), 'ra', axis=0, tiled...  177 us
    all_gather x2, waiting for transfers between devices, per_device(): lax.all_gather(gate_weight[layer].astype(jnp.bfloat16), 'ra', axis=0, til...  119 us
    psum x2, waiting for transfers between devices, per_device(): down = lax.psum(down_part.astype(jnp.bfloat16), 'cb').astype(jnp.float32)  97.4 us
    all_to_all x1, waiting for transfers between devices, per_device(): lax.all_to_all(tokens, 'ra', split_axis=1, concat_axis=0, tiled=True)  97 us
    all_to_all x1, blocking collectives, per_device(): lax.all_to_all(state.T, 'ra', split_axis=0, concat_axis=1, tiled=True)  53.4 us
    dot_general x2, matrix products, per_device(): lax.dot_general(hidden, lax.all_gather(down_weight[layer].astype(jnp.bflo...  27.4 us
  transfers between devices with their start and end apart: 13, of which 9 were waited for; matrix products, arithmetic and copies ran while one was open for 4% of the time, Pallas kernels for 0%

commit v1 on v0

v1 whole, which is shorter than its diff:
```python
import jax
import jax.numpy as jnp
from jax import lax
from jax.sharding import PartitionSpec as P


EPS = 1e-06
RESIDUAL = 0.5


def swap(value, axis, bit):
    count = lax.axis_size(axis)
    return lax.ppermute(value, axis, [(source, source ^ bit) for source in range(count)])


def doublings(low, high):
    bits = []
    while low < high:
        bits.append(low)
        low *= 2
    return bits


def valid_taps(values, taps):
    width = taps.shape[0]
    length = values.shape[0] - width + 1
    total = taps[0][None, :] * values[0:length]
    for k in range(1, width):
        total = total + taps[k][None, :] * values[k : k + length]
    return total


def per_device(
    tokens,
    norm_gain,
    up_weight,
    gate_weight,
    up_scale,
    gate_scale,
    up_taps,
    gate_taps,
    down_weight,
    down_scale,
):
    n_ra, n_cb = lax.axis_size("ra"), lax.axis_size("cb")
    n_y = 1 << ((n_ra.bit_length() - 1) // 2)
    r, j = lax.axis_index("ra"), lax.axis_index("cb")
    layers, rows, columns = up_weight.shape
    half = columns // 2
    members = 2 * n_cb
    groups = n_ra // 2
    length = tokens.shape[1]
    group_tokens = length // groups
    own_tokens = group_tokens // members
    member = (r // n_y) % 2

    steps = [("cb", bit, (j // bit) % 2) for bit in doublings(1, n_cb)] + [("ra", n_y, member)]

    far_bits = doublings(2 * n_y, n_ra) + doublings(1, n_y)
    chunk_offsets = [0]
    for bit in far_bits:
        chunk_offsets += [offset ^ bit for offset in chunk_offsets]
    order = [offset ^ low for offset in chunk_offsets for low in (0, n_y)]
    order_ids = jnp.array(order, jnp.int32) ^ r

    def first_token(device):
        z, y = device // n_y, device % n_y
        group = (z // 2) * n_y + y
        sub = 0
        for axis, bit, mine in steps:
            sub = sub * 2 + (mine if axis == "cb" else z % 2)
        return group * group_tokens + sub * own_tokens

    def collect(weight):
        weight = weight.astype(jnp.bfloat16)
        keep = lax.dynamic_slice_in_dim(weight, member * half, half, 1)
        give = lax.dynamic_slice_in_dim(weight, (1 - member) * half, half, 1)
        chunks = [jnp.concatenate([keep, swap(give, "ra", n_y)], axis=0)]
        for bit in far_bits:
            chunks = chunks + [swap(chunk, "ra", bit) for chunk in chunks]
        return chunks

    def other_order(value):
        parts = jnp.split(value, n_ra, axis=1)
        return jnp.concatenate([parts[k ^ 1] for k in range(n_ra)], axis=1)

    def mine_of(vector):
        return lax.dynamic_slice_in_dim(vector, member * half, half, vector.ndim - 1)

    def by_order(vector):
        return vector.reshape(n_ra, rows)[order_ids].reshape(-1)

    def along_group(value):
        for axis, bit, mine in reversed(steps):
            arrived = swap(value, axis, bit)
            if axis == "ra":
                arrived = other_order(arrived)
            value = jnp.where(
                mine == 0,
                jnp.concatenate([value, arrived], axis=0),
                jnp.concatenate([arrived, value], axis=0),
            )
        return value

    def sum_over_group(value):
        for axis, bit, mine in steps:
            count = value.shape[0] // 2
            keep = lax.dynamic_slice_in_dim(value, mine * count, count, 0)
            give = lax.dynamic_slice_in_dim(value, (1 - mine) * count, count, 0)
            arrived = swap(give.astype(jnp.bfloat16), axis, bit)
            if axis == "ra":
                arrived = other_order(arrived)
            value = keep + arrived.astype(jnp.float32)
        return value

    def from_previous(value):
        pairs = []
        for source in range(n_ra):
            z, y = source // n_y, source % n_y
            group = (z // 2) * n_y + y + 1
            if group < groups:
                pairs.append((source, ((group // n_y) * 2 + z % 2) * n_y + group % n_y))
        return lax.ppermute(value, "ra", pairs)

    pieces = []
    for offset in order:
        piece = lax.dynamic_slice_in_dim(tokens, first_token(r ^ offset), own_tokens, 1)
        pieces.append(swap(piece, "ra", offset) if offset else piece)
    state = jnp.concatenate(pieces, axis=0).T
    weights = [
        [collect(weight[layer]) for weight in (up_weight, gate_weight, down_weight)]
        for layer in range(layers)
    ]
    edge = up_taps.shape[1] - 1
    span = 2 * rows
    for layer in range(layers):
        up, gate, down = weights[layer]
        group_state = along_group(state).astype(jnp.float32)
        inverse = lax.rsqrt(jnp.mean(group_state * group_state, axis=1, keepdims=True) + EPS)
        scaled = (group_state * by_order(norm_gain[layer])[None, :]).astype(jnp.bfloat16)

        def product(chunks):
            total = None
            for k, chunk in enumerate(chunks):
                term = jnp.dot(
                    scaled[:, k * span : (k + 1) * span],
                    chunk,
                    preferred_element_type=jnp.float32,
                )
                total = term if total is None else total + term
            return total

        up_pre = product(up) * inverse * mine_of(up_scale[layer])[None, :]
        gate_pre = product(gate) * inverse * mine_of(gate_scale[layer])[None, :]
        tail = jnp.concatenate([up_pre[-edge:], gate_pre[-edge:]], axis=1)
        before = from_previous(tail)
        conv_up = valid_taps(
            jnp.concatenate([before[:, :half], up_pre], axis=0), mine_of(up_taps[layer])
        )
        conv_gate = valid_taps(
            jnp.concatenate([before[:, half:], gate_pre], axis=0), mine_of(gate_taps[layer])
        )
        hidden = (jax.nn.silu(conv_gate) * conv_up).astype(jnp.bfloat16)
        partial = jnp.concatenate(
            [
                lax.dot_general(
                    hidden,
                    chunk,
                    (((1,), (1,)), ((), ())),
                    preferred_element_type=jnp.float32,
                )
                for chunk in down
            ],
            axis=1,
        )
        total = sum_over_group(partial)
        state = (
            total * by_order(down_scale[layer])[None, :] + RESIDUAL * state.astype(jnp.float32)
        ).astype(jnp.bfloat16)

    turned = state.T.reshape(n_ra, rows, own_tokens)
    pieces = [
        swap(turned[k], "ra", offset) if offset else turned[k] for k, offset in enumerate(order)
    ]
    place = [order.index(k) for k in range(n_ra)]
    stacked = jnp.stack([pieces[k] for k in place])[jnp.arange(n_ra, dtype=jnp.int32) ^ r][None]
    for bit in reversed(doublings(1, n_cb)):
        arrived = swap(stacked, "cb", bit)
        stacked = jnp.where(
            (j // bit) % 2 == 0,
            jnp.concatenate([stacked, arrived], axis=0),
            jnp.concatenate([arrived, stacked], axis=0),
        )
    bits = len(doublings(1, n_cb))
    full = stacked.reshape((2,) * bits + (groups // n_y, 2, n_y, rows, own_tokens))
    axes = (bits + 3, bits, bits + 2) + tuple(range(bits)) + (bits + 1, bits + 4)
    return full.transpose(axes).reshape(rows, length)


def solution(mesh):
    placed = (
        P("ra", None),
        P(),
        P(None, "ra", "cb"),
        P(None, "ra", "cb"),
        P(None, "cb"),
        P(None, "cb"),
        P(None, None, "cb"),
        P(None, None, "cb"),
        P(None, "ra", "cb"),
        P(),
    )

    return jax.shard_map(
        per_device, mesh=mesh, in_specs=placed, out_specs=P("ra", None), check_vma=False
    )
```

time: 838 us -> 589 us (0.70)
  waiting for transfers between devices: 671 us -> 402 us
  blocking collectives: 53.4 us -> 0 us
  starting transfers between devices: 17 us -> 62.2 us
  other arithmetic: 9.65 us -> 46.6 us
  matrix products: 52 us -> 34.6 us
  local copies, waits for them, and re-layouts: 20.3 us -> 36.3 us
  between operations: 13.8 us -> 1.28 us
    all_gather x6 -> x0, waiting for transfers between devices: 475 us -> none  [the longest x2 179 us: per_device(): lax.all_gather(down_weight[layer].astype(jnp.bfloat16), 'ra', axis=0, til...]
    ppermute x4 -> x54, waiting for transfers between devices: 0.01 us -> 402 us  [the longest x52 402 us: swap(): lax.ppermute(value, axis, [(source, source ^ bit) for source in range(cou...]
    psum x2 -> x0, waiting for transfers between devices: 97.4 us -> none  [per_device(): down = lax.psum(down_part.astype(jnp.bfloat16), 'cb').astype(jnp.float32)]
    all_to_all x1 -> x0, waiting for transfers between devices: 97 us -> none  [per_device(): lax.all_to_all(tokens, 'ra', split_axis=1, concat_axis=0, tiled=True)]
    all_to_all x1 -> x0, blocking collectives: 53.4 us -> none  [per_device(): lax.all_to_all(state.T, 'ra', split_axis=0, concat_axis=1, tiled=True)]
    ppermute x4 -> x54, starting transfers between devices: 9.25 us -> 62.2 us  [the longest x52 57.3 us: swap(): lax.ppermute(value, axis, [(source, source ^ bit) for source in range(cou...]
    dot_general x6 -> x24, matrix products: 52 us -> 34.6 us  [the longest x16 23.4 us: product(): jnp.dot(scaled[:, k * span:(k + 1) * span], chunk, preferred_element_type...]
    concatenate x0 -> x10, other arithmetic: none -> 12.8 us  [the longest x6 9.26 us: collect(): chunks = [jnp.concatenate([keep, swap(give, 'ra', n_y)], axis=0)]]
  transfers between devices with their start and end apart: 13 -> 54, of which waited for: 9 -> 32; matrix products, arithmetic and copies ran while one was open for 4% -> 14% of each run, Pallas kernels for 0% -> 0%
where the time goes in v1:
time: 589 us; the launch traced here: 583 us
  waiting for transfers between devices  402 us (68%)
  starting transfers between devices  62.2 us (11%)
  other arithmetic  46.6 us (8%)
  local copies, waits for them, and re-layouts  36.3 us (6%)
  matrix products  34.6 us (6%)
    ppermute x52, waiting for transfers between devices, swap(): lax.ppermute(value, axis, [(source, source ^ bit) for source in range(cou...  402 us
    ppermute x52, starting transfers between devices, swap(): lax.ppermute(value, axis, [(source, source ^ bit) for source in range(cou...  57.3 us
    dot_general x16, matrix products, product(): jnp.dot(scaled[:, k * span:(k + 1) * span], chunk, preferred_element_type...  23.4 us
    unnamed x81, local copies, waits for them, and re-layouts  13.3 us
  transfers between devices with their start and end apart: 54, of which 32 were waited for; matrix products, arithmetic and copies ran while one was open for 14% of the time, Pallas kernels for 0%

profile of v1, /device:TPU:0, one launch (start us, length us, event | category | flops | bytes accessed | tf_op | source)
XLA Modules:
  0.0 583.2 jit_solution(16921836459659956459)
XLA Ops:
  1.1 3.2 collective-permute-start
  4.3 2.6 collective-permute-start.1
  11.3 4.5 collective-permute-start.5
  16.1 2.7 collective-permute-done.5
  18.8 4.9 collective-permute-done.6
  29.6 8.9 %collective-permute-done.7 = bf16[128,2048]{0,1:T(8,128)(2,1)S(1)} collective-permute-done((bf16[128,2048]{0,1:T(8,128)(2,1)S(1)}, bf16[128,2048]{0,1:T(8,128)(2,1)S(1)}, u32[]{:S(2)}, u32[]{:S(2)}) %collective-permute-start.7) | collective-permute-done | bytes 524320 | tf_op jit(solution)/shard_map/ppermute | solution.py:13
  46.7 8.5 %collective-permute-done.8 = bf16[256,2048]{0,1:T(8,128)(2,1)} collective-permute-done((bf16[256,2048]{0,1:T(8,128)(2,1)S(1)}, bf16[256,2048]{0,1:T(8,128)(2,1)}, u32[]{:S(2)}, u32[]{:S(2)}) %collective-permute-start.8) | collective-permute-done | bytes 1048608 | tf_op jit(solution)/shard_map/ppermute | solution.py:13
  73.1 43.3 %collective-permute-done.11 = bf16[512,768]{1,0:T(8,128)(2,1)S(1)} collective-permute-done((bf16[512,768]{1,0:T(8,128)(2,1)}, bf16[512,768]{1,0:T(8,128)(2,1)S(1)}, u32[]{:S(2)}, u32[]{:S(2)}) %collective-permute-start.11) | collective-permute-done | bytes 786464 | tf_op jit(solution)/shard_map/ppermute | solution.py:13
  116.4 33.8 %collective-permute-done.15 = bf16[512,768]{1,0:T(8,128)(2,1)} collective-permute-done((bf16[512,768]{1,0:T(8,128)(2,1)}, bf16[512,768]{1,0:T(8,128)(2,1)}, u32[]{:S(2)}, u32[]{:S(2)}) %collective-permute-start.15) | collective-permute-done | bytes 786464 | tf_op jit(solution)/shard_map/ppermute | solution.py:13
  152.3 4.3 fusion.1
  157.6 2.2 fusion.48
  165.9 4.7 collective-permute-done.13
  172.1 14.4 %collective-permute-done.17 = bf16[512,768]{1,0:T(8,128)(2,1)S(1)} collective-permute-done((bf16[512,768]{1,0:T(8,128)(2,1)}, bf16[512,768]{1,0:T(8,128)(2,1)S(1)}, u32[]{:S(2)}, u32[]{:S(2)}) %collective-permute-start.17) | collective-permute-done | bytes 786464 | tf_op jit(solution)/shard_map/ppermute | solution.py:13
  189.5 2.4 collective-permute-start.18
  194.2 6.0 %fusion.19 = bf16[1024,768]{1,0:T(8,128)(2,1)S(1)} fusion(f32[2,768]{1,0:T(2,128)S(1)} %get-tuple-element.69, f32[1024,768]{1,0:T(8,128)S(1)} %multiply_multiply_fusion.3, f32[1024,768]{1,0:T(8,128)} %copy-done.2, f32[2,768]{1,0:T(2,128)S(1)} %get-tuple-element.68, f32[768]{0:T(1024)S(1)} %get-tuple-element.77, f32[768]{0:T(1024)S(1)} %get-tuple-element.78, ...), kind=kLoop, calls=%fused_computation.44 | loop fusion | flops 15728640 | bytes 7895040 | tf_op jit(solution)/shard_map/convert_element_type | solution.py:163
  204.3 8.4 %collective-permute-done.21 = bf16[512,768]{1,0:T(8,128)(2,1)S(1)} collective-permute-done((bf16[512,768]{1,0:T(8,128)(2,1)}, bf16[512,768]{1,0:T(8,128)(2,1)S(1)}, u32[]{:S(2)}, u32[]{:S(2)}) %collective-permute-start.21) | collective-permute-done | bytes 786464 | tf_op jit(solution)/shard_map/ppermute | solution.py:13
  213.8 13.8 %collective-permute-done.22 = bf16[512,768]{1,0:T(8,128)(2,1)S(1)} collective-permute-done((bf16[512,768]{1,0:T(8,128)(2,1)}, bf16[512,768]{1,0:T(8,128)(2,1)S(1)}, u32[]{:S(2)}, u32[]{:S(2)}) %collective-permute-start.22) | collective-permute-done | bytes 786464 | tf_op jit(solution)/shard_map/ppermute | solution.py:13
  230.3 3.3 copy-done
  234.0 4.3 collective-permute-done.23
  238.3 3.5 convert_add_fusion.1
  245.5 23.8 %collective-permute-done.24 = bf16[256,2048]{0,1:T(8,128)(2,1)} collective-permute-done((bf16[256,2048]{0,1:T(8,128)(2,1)S(1)}, bf16[256,2048]{0,1:T(8,128)(2,1)}, u32[]{:S(2)}, u32[]{:S(2)}) %collective-permute-start.24) | collective-permute-done | bytes 1048608 | tf_op jit(solution)/shard_map/ppermute | solution.py:13
  272.9 12.8 %collective-permute-done.25 = bf16[128,2048]{0,1:T(8,128)(2,1)} collective-permute-done((bf16[128,2048]{0,1:T(8,128)(2,1)}, bf16[128,2048]{0,1:T(8,128)(2,1)}, u32[]{:S(2)}, u32[]{:S(2)}) %collective-permute-start.25) | collective-permute-done | bytes 524320 | tf_op jit(solution)/shard_map/ppermute | solution.py:13
  293.3 11.9 %collective-permute-done.26 = bf16[128,2048]{0,1:T(8,128)(2,1)S(1)} collective-permute-done((bf16[128,2048]{0,1:T(8,128)(2,1)S(1)}, bf16[128,2048]{0,1:T(8,128)(2,1)S(1)}, u32[]{:S(2)}, u32[]{:S(2)}) %collective-permute-start.26) | collective-permute-done | bytes 524320 | tf_op jit(solution)/shard_map/ppermute | solution.py:13
  307.4 21.1 %collective-permute-done.27 = bf16[256,2048]{0,1:T(8,128)(2,1)S(1)} collective-permute-done((bf16[256,2048]{0,1:T(8,128)(2,1)S(1)}, bf16[256,2048]{0,1:T(8,128)(2,1)S(1)}, u32[]{:S(2)}, u32[]{:S(2)}) %collective-permute-start.27) | collective-permute-done | bytes 1048608 | tf_op jit(solution)/shard_map/ppermute | solution.py:13
  331.4 9.8 %collective-permute-done.29 = bf16[256,768]{1,0:T(8,128)(2,1)S(1)} collective-permute-done((bf16[256,768]{1,0:T(8,128)(2,1)S(1)}, bf16[256,768]{1,0:T(8,128)(2,1)S(1)}, u32[]{:S(2)}, u32[]{:S(2)}) %collective-permute-start.29) | collective-permute-done | bytes 393248 | tf_op jit(solution)/shard_map/ppermute | solution.py:13
  342.3 10.3 %collective-permute-done.33 = bf16[256,768]{1,0:T(8,128)(2,1)S(1)} collective-permute-done((bf16[256,768]{1,0:T(8,128)(2,1)S(1)}, bf16[256,768]{1,0:T(8,128)(2,1)S(1)}, u32[]{:S(2)}, u32[]{:S(2)}) %collective-permute-start.33) | collective-permute-done | bytes 393248 | tf_op jit(solution)/shard_map/ppermute | solution.py:13
  356.0 2.5 collective-permute-start.38
  359.5 30.4 %collective-permute-done.38 = bf16[256,768]{1,0:T(8,128)(2,1)} collective-permute-done((bf16[256,768]{1,0:T(8,128)(2,1)}, bf16[256,768]{1,0:T(8,128)(2,1)}, u32[]{:S(2)}, u32[]{:S(2)}) %collective-permute-start.38) | collective-permute-done | bytes 393248 | tf_op jit(solution)/shard_map/ppermute | solution.py:13
  391.3 23.2 %collective-permute-done.30 = bf16[512,768]{1,0:T(8,128)(2,1)} collective-permute-done((bf16[512,768]{1,0:T(8,128)(2,1)}, bf16[512,768]{1,0:T(8,128)(2,1)}, u32[]{:S(2)}, u32[]{:S(2)}) %collective-permute-start.30) | collective-permute-done | bytes 786464 | tf_op jit(solution)/shard_map/ppermute | solution.py:13
  414.5 16.8 %collective-permute-done.34 = bf16[512,768]{1,0:T(8,128)(2,1)} collective-permute-done((bf16[512,768]{1,0:T(8,128)(2,1)}, bf16[512,768]{1,0:T(8,128)(2,1)}, u32[]{:S(2)}, u32[]{:S(2)}) %collective-permute-start.34) | collective-permute-done | bytes 786464 | tf_op jit(solution)/shard_map/ppermute | solution.py:13
  433.4 4.2 fusion.3
  438.7 2.2 fusion.36
  441.9 10.1 %collective-permute-done.32 = bf16[512,768]{1,0:T(8,128)(2,1)S(1)} collective-permute-done((bf16[512,768]{1,0:T(8,128)(2,1)}, bf16[512,768]{1,0:T(8,128)(2,1)S(1)}, u32[]{:S(2)}, u32[]{:S(2)}) %collective-permute-start.32) | collective-permute-done | bytes 786464 | tf_op jit(solution)/shard_map/ppermute | solution.py:13
  454.5 2.2 fusion.34
  457.7 6.7 %collective-permute-done.36 = bf16[512,768]{1,0:T(8,128)(2,1)S(1)} collective-permute-done((bf16[512,768]{1,0:T(8,128)(2,1)}, bf16[512,768]{1,0:T(8,128)(2,1)S(1)}, u32[]{:S(2)}, u32[]{:S(2)}) %collective-permute-start.36) | collective-permute-done | bytes 786464 | tf_op jit(solution)/shard_map/ppermute | solution.py:13
  465.8 2.4 collective-permute-start.37
  470.4 2.9 fusion.9
  476.4 12.4 %collective-permute-done.40 = bf16[512,768]{1,0:T(8,128)(2,1)S(1)} collective-permute-done((bf16[512,768]{1,0:T(8,128)(2,1)S(1)}, bf16[512,768]{1,0:T(8,128)(2,1)S(1)}, u32[]{:S(2)}, u32[]{:S(2)}) %collective-permute-start.40) | collective-permute-done | bytes 786464 | tf_op jit(solution)/shard_map/ppermute | solution.py:13
  489.8 10.2 %collective-permute-done.41 = bf16[512,768]{1,0:T(8,128)(2,1)S(1)} collective-permute-done((bf16[512,768]{1,0:T(8,128)(2,1)S(1)}, bf16[512,768]{1,0:T(8,128)(2,1)S(1)}, u32[]{:S(2)}, u32[]{:S(2)}) %collective-permute-start.41) | collective-permute-done | bytes 786464 | tf_op jit(solution)/shard_map/ppermute | solution.py:13
  503.2 4.1 collective-permute-done.42
  509.9 23.7 %collective-permute-done.43 = bf16[256,2048]{0,1:T(8,128)(2,1)S(1)} collective-permute-done((bf16[256,2048]{0,1:T(8,128)(2,1)S(1)}, bf16[256,2048]{0,1:T(8,128)(2,1)S(1)}, u32[]{:S(2)}, u32[]{:S(2)}) %collective-permute-start.43) | collective-permute-done | bytes 1048608 | tf_op jit(solution)/shard_map/ppermute | solution.py:13
  536.1 12.0 %collective-permute-done.44 = bf16[128,2048]{0,1:T(8,128)(2,1)S(1)} collective-permute-done((bf16[128,2048]{0,1:T(8,128)(2,1)}, bf16[128,2048]{0,1:T(8,128)(2,1)S(1)}, u32[]{:S(2)}, u32[]{:S(2)}) %collective-permute-start.44) | collective-permute-done | bytes 524320 | tf_op jit(solution)/shard_map/ppermute | solution.py:13
  552.3 3.0 collective-permute-start.49
  556.5 3.5 collective-permute-start.51
  565.9 8.9 %collective-permute-done.52 = bf16[1,8,256,128]{3,2,1,0:T(8,128)(2,1)S(1)} collective-permute-done((bf16[1,8,256,128]{3,2,1,0:T(8,128)(2,1)S(1)}, bf16[1,8,256,128]{3,2,1,0:T(8,128)(2,1)S(1)}, u32[]{:S(2)}, u32[]{:S(2)}) %collective-permute-start.52) | collective-permute-done | bytes 524320 | tf_op jit(solution)/shard_map/ppermute | solution.py:13
  575.0 2.6 collective-permute-done.53
  578.0 2.2 copy.12
  580.1 2.8 reshape.114
  (249 shorter events, 123.5 us)
Async XLA Ops:
  1.1 10.2 %collective-permute-start = (bf16[256,128]{1,0:T(8,128)(2,1)S(1)}, bf16[256,128]{1,0:T(8,128)(2,1)S(1)}, u32[]{:S(2)}, u32[]{:S(2)}) collective-permute-start(bf16[256,128]{1,0:T(8,128)(2,1)S(1)} %get-tuple-element.30), channel_id=1, source_target_pairs={{0,8},{4,12},{8,0},{12,4},{16,24},{20,28},{24,16},{28,20},{1,9},{5... | collective-permute-start | bytes 196616 | tf_op jit(solution)/shard_map/ppermute | solution.py:13
  4.3 11.6 %collective-permute-start.1 = (bf16[256,128]{1,0:T(8,128)(2,1)S(1)}, bf16[256,128]{1,0:T(8,128)(2,1)S(1)}, u32[]{:S(2)}, u32[]{:S(2)}) collective-permute-start(bf16[256,128]{1,0:T(8,128)(2,1)S(1)} %get-tuple-element.29), channel_id=1, source_target_pairs={{0,16},{4,20},{8,24},{12,28},{16,0},{20,4},{24,8},{28,12},{1,17},{... | collective-permute-start | bytes 196616 | tf_op jit(solution)/shard_map/ppermute | solution.py:13
  6.9 9.1 %collective-permute-start.2 = (bf16[256,128]{1,0:T(8,128)(2,1)S(1)}, bf16[256,128]{1,0:T(8,128)(2,1)S(1)}, u32[]{:S(2)}, u32[]{:S(2)}) collective-permute-start(bf16[256,128]{1,0:T(8,128)(2,1)S(1)} %get-tuple-element.28), channel_id=1, source_target_pairs={{0,24},{4,28},{8,16},{12,20},{16,8},{20,12},{24,0},{28,4},{1,25},{... | collective-permute-start | bytes 196616 | tf_op jit(solution)/shard_map/ppermute | solution.py:13
  6.9 9.1 %collective-permute-start.3 = (bf16[256,128]{1,0:T(8,128)(2,1)S(1)}, bf16[256,128]{1,0:T(8,128)(2,1)S(1)}, u32[]{:S(2)}, u32[]{:S(2)}) collective-permute-start(bf16[256,128]{1,0:T(8,128)(2,1)S(1)} %get-tuple-element.27), channel_id=1, source_target_pairs={{0,4},{4,0},{8,12},{12,8},{16,20},{20,16},{24,28},{28,24},{1,5},{5... | collective-permute-start | bytes 196616 | tf_op jit(solution)/shard_map/ppermute | solution.py:13
  8.6 7.4 %collective-permute-start.4 = (bf16[256,128]{1,0:T(8,128)(2,1)S(1)}, bf16[256,128]{1,0:T(8,128)(2,1)S(1)}, u32[]{:S(2)}, u32[]{:S(2)}) collective-permute-start(bf16[256,128]{1,0:T(8,128)(2,1)S(1)} %get-tuple-element.26), channel_id=1, source_target_pairs={{0,12},{4,8},{8,4},{12,0},{16,28},{20,24},{24,20},{28,16},{1,13},{... | collective-permute-start | bytes 196616 | tf_op jit(solution)/shard_map/ppermute | solution.py:13
  11.3 7.4 %collective-permute-start.5 = (bf16[256,128]{1,0:T(8,128)(2,1)S(1)}, bf16[256,128]{1,0:T(8,128)(2,1)S(1)}, u32[]{:S(2)}, u32[]{:S(2)}) collective-permute-start(bf16[256,128]{1,0:T(8,128)(2,1)S(1)} %get-tuple-element.32), channel_id=1, source_target_pairs={{0,20},{4,16},{8,28},{12,24},{16,4},{20,0},{24,12},{28,8},{1,21},{... | collective-permute-start | bytes 196616 | tf_op jit(solution)/shard_map/ppermute | solution.py:13
  15.9 7.7 %collective-permute-start.6 = (bf16[256,128]{1,0:T(8,128)(2,1)S(1)}, bf16[256,128]{1,0:T(8,128)(2,1)S(1)}, u32[]{:S(2)}, u32[]{:S(2)}) collective-permute-start(bf16[256,128]{1,0:T(8,128)(2,1)S(1)} %get-tuple-element.25), channel_id=1, source_target_pairs={{0,28},{4,24},{8,20},{12,16},{16,12},{20,8},{24,4},{28,0},{1,29},{... | collective-permute-start | bytes 196616 | tf_op jit(solution)/shard_map/ppermute | solution.py:13
  23.6 14.9 %collective-permute-start.7 = (bf16[128,2048]{0,1:T(8,128)(2,1)S(1)}, bf16[128,2048]{0,1:T(8,128)(2,1)S(1)}, u32[]{:S(2)}, u32[]{:S(2)}) collective-permute-start(bf16[128,2048]{0,1:T(8,128)(2,1)S(1)} %bitcast.87), channel_id=1, source_target_pairs={{0,8},{4,12},{8,0},{12,4},{16,24},{20,28},{24,16},{28,20},{1,9},{5... | collective-permute-start | bytes 1572872 | tf_op jit(solution)/shard_map/ppermute | solution.py:13
  25.6 34.1 %collective-permute-start.10 = (bf16[256,768]{1,0:T(8,128)(2,1)}, bf16[256,768]{1,0:T(8,128)(2,1)}, u32[]{:S(2)}, u32[]{:S(2)}) collective-permute-start(bf16[256,768]{1,0:T(8,128)(2,1)} %get-tuple-element.48), channel_id=1, source_target_pairs={{0,8},{4,12},{8,0},{12,4},{16,24},{20,28},{24,16},{28,20},{1,9},{5... | collective-permute-start | bytes 1179656 | tf_op jit(solution)/shard_map/ppermute | solution.py:13
  39.1 16.2 %collective-permute-start.8 = (bf16[256,2048]{0,1:T(8,128)(2,1)S(1)}, bf16[256,2048]{0,1:T(8,128)(2,1)}, u32[]{:S(2)}, u32[]{:S(2)}) collective-permute-start(bf16[256,2048]{0,1:T(8,128)(2,1)S(1)} %maximum_select_fusion.5), channel_id=1, source_target_pairs={{0,2},{1,3},{2,0},{3,1},{4,6},{5,7},{6,4},{7,5},{8,10},{9,11},{10,... | collective-permute-start | bytes 3145736 | tf_op jit(solution)/shard_map/ppermute | solution.py:13
  42.6 20.4 %collective-permute-start.14 = (bf16[256,768]{1,0:T(8,128)(2,1)}, bf16[256,768]{1,0:T(8,128)(2,1)}, u32[]{:S(2)}, u32[]{:S(2)}) collective-permute-start(bf16[256,768]{1,0:T(8,128)(2,1)} %get-tuple-element.50), channel_id=1, source_target_pairs={{0,8},{4,12},{8,0},{12,4},{16,24},{20,28},{24,16},{28,20},{1,9},{5... | collective-permute-start | bytes 1179656 | tf_op jit(solution)/shard_map/ppermute | solution.py:13
  44.7 25.8 %collective-permute-start.19 = (bf16[256,768]{1,0:T(8,128)(2,1)}, bf16[256,768]{1,0:T(8,128)(2,1)}, u32[]{:S(2)}, u32[]{:S(2)}) collective-permute-start(bf16[256,768]{1,0:T(8,128)(2,1)} %get-tuple-element.46), channel_id=1, source_target_pairs={{0,8},{4,12},{8,0},{12,4},{16,24},{20,28},{24,16},{28,20},{1,9},{5... | collective-permute-start | bytes 1179656 | tf_op jit(solution)/shard_map/ppermute | solution.py:13
  57.3 93.3 %collective-permute-start.9 = (bf16[512,2048]{0,1:T(8,128)(2,1)S(1)}, bf16[512,2048]{0,1:T(8,128)(2,1)}, u32[]{:S(2)}, u32[]{:S(2)}) collective-permute-start(bf16[512,2048]{0,1:T(8,128)(2,1)S(1)} %maximum_select_fusion.2), channel_id=1, source_target_pairs={{0,1},{1,0},{2,3},{3,2},{4,5},{5,4},{6,7},{7,6},{8,9},{9,8},{10,11... | collective-permute-start | bytes 6291464 | tf_op jit(solution)/shard_map/ppermute | solution.py:13
  61.6 54.9 %collective-permute-start.11 = (bf16[512,768]{1,0:T(8,128)(2,1)}, bf16[512,768]{1,0:T(8,128)(2,1)S(1)}, u32[]{:S(2)}, u32[]{:S(2)}) collective-permute-start(bf16[512,768]{1,0:T(8,128)(2,1)} %pad_maximum_fusion.6), channel_id=1, source_target_pairs={{0,16},{4,20},{8,24},{12,28},{16,0},{20,4},{24,8},{28,12},{1,17},{... | collective-permute-start | bytes 2359304 | tf_op jit(solution)/shard_map/ppermute | solution.py:13
  65.0 85.2 %collective-permute-start.15 = (bf16[512,768]{1,0:T(8,128)(2,1)}, bf16[512,768]{1,0:T(8,128)(2,1)}, u32[]{:S(2)}, u32[]{:S(2)}) collective-permute-start(bf16[512,768]{1,0:T(8,128)(2,1)} %pad_maximum_fusion.7), channel_id=1, source_target_pairs={{0,16},{4,20},{8,24},{12,28},{16,0},{20,4},{24,8},{28,12},{1,17},{... | collective-permute-start | bytes 2359304 | tf_op jit(solution)/shard_map/ppermute | solution.py:13
  69.0 92.8 %collective-permute-start.12 = (bf16[512,768]{1,0:T(8,128)(2,1)}, bf16[512,768]{1,0:T(8,128)(2,1)S(1)}, u32[]{:S(2)}, u32[]{:S(2)}) collective-permute-start(bf16[512,768]{1,0:T(8,128)(2,1)} %pad_maximum_fusion.6), channel_id=1, source_target_pairs={{0,4},{4,0},{8,12},{12,8},{16,20},{20,16},{24,28},{28,24},{1,5},{5... | collective-permute-start | bytes 2359304 | tf_op jit(solution)/shard_map/ppermute | solution.py:13
  70.5 94.4 %collective-permute-start.16 = (bf16[512,768]{1,0:T(8,128)(2,1)}, bf16[512,768]{1,0:T(8,128)(2,1)S(1)}, u32[]{:S(2)}, u32[]{:S(2)}) collective-permute-start(bf16[512,768]{1,0:T(8,128)(2,1)} %pad_maximum_fusion.7), channel_id=1, source_target_pairs={{0,4},{4,0},{8,12},{12,8},{16,20},{20,16},{24,28},{28,24},{1,5},{5... | collective-permute-start | bytes 2359304 | tf_op jit(solution)/shard_map/ppermute | solution.py:13
  116.4 76.2 %collective-permute-start.20 = (bf16[512,768]{1,0:T(8,128)(2,1)}, bf16[512,768]{1,0:T(8,128)(2,1)}, u32[]{:S(2)}, u32[]{:S(2)}) collective-permute-start(bf16[512,768]{1,0:T(8,128)(2,1)} %pad_maximum_fusion.8), channel_id=1, source_target_pairs={{0,16},{4,20},{8,24},{12,28},{16,0},{20,4},{24,8},{28,12},{1,17},{... | collective-permute-start | bytes 2359304 | tf_op jit(solution)/shard_map/ppermute | solution.py:13
  150.3 20.4 %collective-permute-start.13 = (bf16[512,768]{1,0:T(8,128)(2,1)S(1)}, bf16[512,768]{1,0:T(8,128)(2,1)S(1)}, u32[]{:S(2)}, u32[]{:S(2)}) collective-permute-start(bf16[512,768]{1,0:T(8,128)(2,1)S(1)} %collective-permute-done.11), channel_id=1, source_target_pairs={{0,4},{4,0},{8,12},{12,8},{16,20},{20,16},{24,28},{28,24},{1,5},{5... | collective-permute-start | bytes 2359304 | tf_op jit(solution)/shard_map/ppermute | solution.py:13
  150.6 35.8 %collective-permute-start.17 = (bf16[512,768]{1,0:T(8,128)(2,1)}, bf16[512,768]{1,0:T(8,128)(2,1)S(1)}, u32[]{:S(2)}, u32[]{:S(2)}) collective-permute-start(bf16[512,768]{1,0:T(8,128)(2,1)} %collective-permute-done.15), channel_id=1, source_target_pairs={{0,4},{4,0},{8,12},{12,8},{16,20},{20,16},{24,28},{28,24},{1,5},{5... | collective-permute-start | bytes 2359304 | tf_op jit(solution)/shard_map/ppermute | solution.py:13
  192.1 20.7 %collective-permute-start.21 = (bf16[512,768]{1,0:T(8,128)(2,1)}, bf16[512,768]{1,0:T(8,128)(2,1)S(1)}, u32[]{:S(2)}, u32[]{:S(2)}) collective-permute-start(bf16[512,768]{1,0:T(8,128)(2,1)} %pad_maximum_fusion.8), channel_id=1, source_target_pairs={{0,4},{4,0},{8,12},{12,8},{16,20},{20,16},{24,28},{28,24},{1,5},{5... | collective-permute-start | bytes 2359304 | tf_op jit(solution)/shard_map/ppermute | solution.py:13
  192.7 34.9 %collective-permute-start.22 = (bf16[512,768]{1,0:T(8,128)(2,1)}, bf16[512,768]{1,0:T(8,128)(2,1)S(1)}, u32[]{:S(2)}, u32[]{:S(2)}) collective-permute-start(bf16[512,768]{1,0:T(8,128)(2,1)} %collective-permute-done.20), channel_id=1, source_target_pairs={{0,4},{4,0},{8,12},{12,8},{16,20},{20,16},{24,28},{28,24},{1,5},{5... | collective-permute-start | bytes 2359304 | tf_op jit(solution)/shard_map/ppermute | solution.py:13
  243.9 25.4 %collective-permute-start.24 = (bf16[256,2048]{0,1:T(8,128)(2,1)S(1)}, bf16[256,2048]{0,1:T(8,128)(2,1)}, u32[]{:S(2)}, u32[]{:S(2)}) collective-permute-start(bf16[256,2048]{0,1:T(8,128)(2,1)S(1)} %dynamic-slice_convert_fusion.3), channel_id=1, source_target_pairs={{0,2},{1,3},{2,0},{3,1},{4,6},{5,7},{6,4},{7,5},{8,10},{9,11},{10,... | collective-permute-start | bytes 3145736 | tf_op jit(solution)/shard_map/ppermute | solution.py:13
  272.3 13.4 %collective-permute-start.25 = (bf16[128,2048]{0,1:T(8,128)(2,1)}, bf16[128,2048]{0,1:T(8,128)(2,1)}, u32[]{:S(2)}, u32[]{:S(2)}) collective-permute-start(bf16[128,2048]{0,1:T(8,128)(2,1)} %dynamic-slice_convert_fusion.5), channel_id=1, source_target_pairs={{0,8},{4,12},{8,0},{12,4},{16,24},{20,28},{24,16},{28,20},{1,9},{5... | collective-permute-start | bytes 1572872 | tf_op jit(solution)/shard_map/ppermute | solution.py:13
  292.9 12.3 %collective-permute-start.26 = (bf16[128,2048]{0,1:T(8,128)(2,1)S(1)}, bf16[128,2048]{0,1:T(8,128)(2,1)S(1)}, u32[]{:S(2)}, u32[]{:S(2)}) collective-permute-start(bf16[128,2048]{0,1:T(8,128)(2,1)S(1)} %add_convert_fusion.1), channel_id=1, source_target_pairs={{0,8},{4,12},{8,0},{12,4},{16,24},{20,28},{24,16},{28,20},{1,9},{5... | collective-permute-start | bytes 1572872 | tf_op jit(solution)/shard_map/ppermute | solution.py:13
  305.8 22.7 %collective-permute-start.27 = (bf16[256,2048]{0,1:T(8,128)(2,1)S(1)}, bf16[256,2048]{0,1:T(8,128)(2,1)S(1)}, u32[]{:S(2)}, u32[]{:S(2)}) collective-permute-start(bf16[256,2048]{0,1:T(8,128)(2,1)S(1)} %maximum_select_fusion.6), channel_id=1, source_target_pairs={{0,2},{1,3},{2,0},{3,1},{4,6},{5,7},{6,4},{7,5},{8,10},{9,11},{10,... | collective-permute-start | bytes 3145736 | tf_op jit(solution)/shard_map/ppermute | solution.py:13
  329.0 102.8 %collective-permute-start.28 = (bf16[512,2048]{0,1:T(8,128)(2,1)S(1)}, bf16[512,2048]{0,1:T(8,128)(2,1)}, u32[]{:S(2)}, u32[]{:S(2)}) collective-permute-start(bf16[512,2048]{0,1:T(8,128)(2,1)S(1)} %maximum_select_fusion.3), channel_id=1, source_target_pairs={{0,1},{1,0},{2,3},{3,2},{4,5},{5,4},{6,7},{7,6},{8,9},{9,8},{10,11... | collective-permute-start | bytes 6291464 | tf_op jit(solution)/shard_map/ppermute | solution.py:13
  329.2 12.1 %collective-permute-start.29 = (bf16[256,768]{1,0:T(8,128)(2,1)S(1)}, bf16[256,768]{1,0:T(8,128)(2,1)S(1)}, u32[]{:S(2)}, u32[]{:S(2)}) collective-permute-start(bf16[256,768]{1,0:T(8,128)(2,1)S(1)} %get-tuple-element.42), channel_id=1, source_target_pairs={{0,8},{4,12},{8,0},{12,4},{16,24},{20,28},{24,16},{28,20},{1,9},{5... | collective-permute-start | bytes 1179656 | tf_op jit(solution)/shard_map/ppermute | solution.py:13
  330.2 22.4 %collective-permute-start.33 = (bf16[256,768]{1,0:T(8,128)(2,1)S(1)}, bf16[256,768]{1,0:T(8,128)(2,1)S(1)}, u32[]{:S(2)}, u32[]{:S(2)}) collective-permute-start(bf16[256,768]{1,0:T(8,128)(2,1)S(1)} %get-tuple-element.44), channel_id=1, source_target_pairs={{0,8},{4,12},{8,0},{12,4},{16,24},{20,28},{24,16},{28,20},{1,9},{5... | collective-permute-start | bytes 1179656 | tf_op jit(solution)/shard_map/ppermute | solution.py:13
  342.3 72.2 %collective-permute-start.30 = (bf16[512,768]{1,0:T(8,128)(2,1)}, bf16[512,768]{1,0:T(8,128)(2,1)}, u32[]{:S(2)}, u32[]{:S(2)}) collective-permute-start(bf16[512,768]{1,0:T(8,128)(2,1)} %pad_maximum_fusion.9), channel_id=1, source_target_pairs={{0,16},{4,20},{8,24},{12,28},{16,0},{20,4},{24,8},{28,12},{1,17},{... | collective-permute-start | bytes 2359304 | tf_op jit(solution)/shard_map/ppermute | solution.py:13
  353.6 77.8 %collective-permute-start.34 = (bf16[512,768]{1,0:T(8,128)(2,1)}, bf16[512,768]{1,0:T(8,128)(2,1)}, u32[]{:S(2)}, u32[]{:S(2)}) collective-permute-start(bf16[512,768]{1,0:T(8,128)(2,1)} %pad_maximum_fusion.10), channel_id=1, source_target_pairs={{0,16},{4,20},{8,24},{12,28},{16,0},{20,4},{24,8},{28,12},{1,17},{... | collective-permute-start | bytes 2359304 | tf_op jit(solution)/shard_map/ppermute | solution.py:13
  356.0 33.8 %collective-permute-start.38 = (bf16[256,768]{1,0:T(8,128)(2,1)}, bf16[256,768]{1,0:T(8,128)(2,1)}, u32[]{:S(2)}, u32[]{:S(2)}) collective-permute-start(bf16[256,768]{1,0:T(8,128)(2,1)} %get-tuple-element.40), channel_id=1, source_target_pairs={{0,8},{4,12},{8,0},{12,4},{16,24},{20,28},{24,16},{28,20},{1,9},{5... | collective-permute-start | bytes 1179656 | tf_op jit(solution)/shard_map/ppermute | solution.py:13
  359.1 81.7 %collective-permute-start.31 = (bf16[512,768]{1,0:T(8,128)(2,1)}, bf16[512,768]{1,0:T(8,128)(2,1)S(1)}, u32[]{:S(2)}, u32[]{:S(2)}) collective-permute-start(bf16[512,768]{1,0:T(8,128)(2,1)} %pad_maximum_fusion.9), channel_id=1, source_target_pairs={{0,4},{4,0},{8,12},{12,8},{16,20},{20,16},{24,28},{28,24},{1,5},{5... | collective-permute-start | bytes 2359304 | tf_op jit(solution)/shard_map/ppermute | solution.py:13
  389.9 66.8 %collective-permute-start.35 = (bf16[512,768]{1,0:T(8,128)(2,1)}, bf16[512,768]{1,0:T(8,128)(2,1)S(1)}, u32[]{:S(2)}, u32[]{:S(2)}) collective-permute-start(bf16[512,768]{1,0:T(8,128)(2,1)} %pad_maximum_fusion.10), channel_id=1, source_target_pairs={{0,4},{4,0},{8,12},{12,8},{16,20},{20,16},{24,28},{28,24},{1,5},{5... | collective-permute-start | bytes 2359304 | tf_op jit(solution)/shard_map/ppermute | solution.py:13
  414.5 54.4 %collective-permute-start.39 = (bf16[512,768]{1,0:T(8,128)(2,1)S(1)}, bf16[512,768]{1,0:T(8,128)(2,1)S(1)}, u32[]{:S(2)}, u32[]{:S(2)}) collective-permute-start(bf16[512,768]{1,0:T(8,128)(2,1)S(1)} %pad_maximum_fusion.11), channel_id=1, source_target_pairs={{0,16},{4,20},{8,24},{12,28},{16,0},{20,4},{24,8},{28,12},{1,17},{... | collective-permute-start | bytes 2359304 | tf_op jit(solution)/shard_map/ppermute | solution.py:13
  431.4 20.6 %collective-permute-start.32 = (bf16[512,768]{1,0:T(8,128)(2,1)}, bf16[512,768]{1,0:T(8,128)(2,1)S(1)}, u32[]{:S(2)}, u32[]{:S(2)}) collective-permute-start(bf16[512,768]{1,0:T(8,128)(2,1)} %collective-permute-done.30), channel_id=1, source_target_pairs={{0,4},{4,0},{8,12},{12,8},{16,20},{20,16},{24,28},{28,24},{1,5},{5... | collective-permute-start | bytes 2359304 | tf_op jit(solution)/shard_map/ppermute | solution.py:13
  431.9 32.5 %collective-permute-start.36 = (bf16[512,768]{1,0:T(8,128)(2,1)}, bf16[512,768]{1,0:T(8,128)(2,1)S(1)}, u32[]{:S(2)}, u32[]{:S(2)}) collective-permute-start(bf16[512,768]{1,0:T(8,128)(2,1)} %collective-permute-done.34), channel_id=1, source_target_pairs={{0,4},{4,0},{8,12},{12,8},{16,20},{20,16},{24,28},{28,24},{1,5},{5... | collective-permute-start | bytes 2359304 | tf_op jit(solution)/shard_map/ppermute | solution.py:13
  468.3 20.5 %collective-permute-start.40 = (bf16[512,768]{1,0:T(8,128)(2,1)S(1)}, bf16[512,768]{1,0:T(8,128)(2,1)S(1)}, u32[]{:S(2)}, u32[]{:S(2)}) collective-permute-start(bf16[512,768]{1,0:T(8,128)(2,1)S(1)} %pad_maximum_fusion.11), channel_id=1, source_target_pairs={{0,4},{4,0},{8,12},{12,8},{16,20},{20,16},{24,28},{28,24},{1,5},{5... | collective-permute-start | bytes 2359304 | tf_op jit(solution)/shard_map/ppermute | solution.py:13
  468.9 31.2 %collective-permute-start.41 = (bf16[512,768]{1,0:T(8,128)(2,1)S(1)}, bf16[512,768]{1,0:T(8,128)(2,1)S(1)}, u32[]{:S(2)}, u32[]{:S(2)}) collective-permute-start(bf16[512,768]{1,0:T(8,128)(2,1)S(1)} %collective-permute-done.39), channel_id=1, source_target_pairs={{0,4},{4,0},{8,12},{12,8},{16,20},{20,16},{24,28},{28,24},{1,5},{5... | collective-permute-start | bytes 2359304 | tf_op jit(solution)/shard_map/ppermute | solution.py:13
  508.3 25.3 %collective-permute-start.43 = (bf16[256,2048]{0,1:T(8,128)(2,1)S(1)}, bf16[256,2048]{0,1:T(8,128)(2,1)S(1)}, u32[]{:S(2)}, u32[]{:S(2)}) collective-permute-start(bf16[256,2048]{0,1:T(8,128)(2,1)S(1)} %dynamic-slice_convert_fusion.2), channel_id=1, source_target_pairs={{0,2},{1,3},{2,0},{3,1},{4,6},{5,7},{6,4},{7,5},{8,10},{9,11},{10,... | collective-permute-start | bytes 3145736 | tf_op jit(solution)/shard_map/ppermute | solution.py:13
  534.8 13.3 %collective-permute-start.44 = (bf16[128,2048]{0,1:T(8,128)(2,1)}, bf16[128,2048]{0,1:T(8,128)(2,1)S(1)}, u32[]{:S(2)}, u32[]{:S(2)}) collective-permute-start(bf16[128,2048]{0,1:T(8,128)(2,1)} %dynamic-slice_convert_fusion.4), channel_id=1, source_target_pairs={{0,8},{4,12},{8,0},{12,4},{16,24},{20,28},{24,16},{28,20},{1,9},{5... | collective-permute-start | bytes 1572872 | tf_op jit(solution)/shard_map/ppermute | solution.py:13
  549.4 7.1 %collective-permute-start.46 = (bf16[256,128]{1,0:T(8,128)(2,1)S(1)}, bf16[256,128]{1,0:T(8,128)(2,1)S(1)}, u32[]{:S(2)}, u32[]{:S(2)}) collective-permute-start(bf16[256,128]{1,0:T(8,128)(2,1)S(1)} %get-tuple-element.56), channel_id=1, source_target_pairs={{0,8},{4,12},{8,0},{12,4},{16,24},{20,28},{24,16},{28,20},{1,9},{5... | collective-permute-start | bytes 196616 | tf_op jit(solution)/shard_map/ppermute | solution.py:13
  551.2 8.8 %collective-permute-start.47 = (bf16[256,128]{1,0:T(8,128)(2,1)S(1)}, bf16[256,128]{1,0:T(8,128)(2,1)S(1)}, u32[]{:S(2)}, u32[]{:S(2)}) collective-permute-start(bf16[256,128]{1,0:T(8,128)(2,1)S(1)} %get-tuple-element.55), channel_id=1, source_target_pairs={{0,12},{4,8},{8,4},{12,0},{16,28},{20,24},{24,20},{28,16},{1,13},{... | collective-permute-start | bytes 196616 | tf_op jit(solution)/shard_map/ppermute | solution.py:13
  552.3 9.4 %collective-permute-start.48 = (bf16[256,128]{1,0:T(8,128)(2,1)S(1)}, bf16[256,128]{1,0:T(8,128)(2,1)S(1)}, u32[]{:S(2)}, u32[]{:S(2)}) collective-permute-start(bf16[256,128]{1,0:T(8,128)(2,1)S(1)} %get-tuple-element.54), channel_id=1, source_target_pairs={{0,16},{4,20},{8,24},{12,28},{16,0},{20,4},{24,8},{28,12},{1,17},{... | collective-permute-start | bytes 196616 | tf_op jit(solution)/shard_map/ppermute | solution.py:13
  552.3 10.7 %collective-permute-start.49 = (bf16[256,128]{1,0:T(8,128)(2,1)S(1)}, bf16[256,128]{1,0:T(8,128)(2,1)S(1)}, u32[]{:S(2)}, u32[]{:S(2)}) collective-permute-start(bf16[256,128]{1,0:T(8,128)(2,1)S(1)} %get-tuple-element.53), channel_id=1, source_target_pairs={{0,20},{4,16},{8,28},{12,24},{16,4},{20,0},{24,12},{28,8},{1,21},{... | collective-permute-start | bytes 196616 | tf_op jit(solution)/shard_map/ppermute | solution.py:13
  555.3 7.6 %collective-permute-start.50 = (bf16[256,128]{1,0:T(8,128)(2,1)S(1)}, bf16[256,128]{1,0:T(8,128)(2,1)S(1)}, u32[]{:S(2)}, u32[]{:S(2)}) collective-permute-start(bf16[256,128]{1,0:T(8,128)(2,1)S(1)} %get-tuple-element.52), channel_id=1, source_target_pairs={{0,24},{4,28},{8,16},{12,20},{16,8},{20,12},{24,0},{28,4},{1,25},{... | collective-permute-start | bytes 196616 | tf_op jit(solution)/shard_map/ppermute | solution.py:13
  556.5 7.1 %collective-permute-start.51 = (bf16[256,128]{1,0:T(8,128)(2,1)S(1)}, bf16[256,128]{1,0:T(8,128)(2,1)S(1)}, u32[]{:S(2)}, u32[]{:S(2)}) collective-permute-start(bf16[256,128]{1,0:T(8,128)(2,1)S(1)} %get-tuple-element.51), channel_id=1, source_target_pairs={{0,28},{4,24},{8,20},{12,16},{16,12},{20,8},{24,4},{28,0},{1,29},{... | collective-permute-start | bytes 196616 | tf_op jit(solution)/shard_map/ppermute | solution.py:13
  564.3 10.4 %collective-permute-start.52 = (bf16[1,8,256,128]{3,2,1,0:T(8,128)(2,1)S(1)}, bf16[1,8,256,128]{3,2,1,0:T(8,128)(2,1)S(1)}, u32[]{:S(2)}, u32[]{:S(2)}) collective-permute-start(bf16[1,8,256,128]{3,2,1,0:T(8,128)(2,1)S(1)} %bitcast.89), channel_id=1, source_target_pairs={{0,2},{1,3},{2,0},{3,1},{4,6},{5,7},{6,4},{7,5},{8,10},{9,11},{10,... | collective-permute-start | bytes 1572872 | tf_op jit(solution)/shard_map/ppermute | solution.py:13
  (24 other events, 233.3 us)
